TPU v7x, 32 devices: a whole 2x2x4 slice. The times are simulated.
32 devices in a mesh: fs: 4 (over y, x), tp: 8 (over z, core).
Axes of the slice: x: 2, y: 2, z: 4, core: 2. Of those that a mesh axis runs over, the one named last changes fastest.
Arguments:
- value_input: bfloat16 [8192, 2048], P('fs', 'tp'), may hold values from -50 to 50
- value_cotangent: bfloat16 [8192, 512], P('fs'), may hold values from -6 to 6
- value_factor: bfloat16 [512, 128], replicated, may hold values from -10 to 10
- value_master: float32 [512, 2048], P('fs', 'tp'), may hold values from -0.125 to 0.125
- value_first: float32 [128, 2048], P('fs', 'tp'), may hold values from -4 to 4
- value_second: float32 [128, 2048], P('fs', 'tp'), may hold values from 0.01 to 0.2
- mixed_heads: bfloat16 [8192, 1024], P('fs', 'tp'), may hold values from -6 to 6
- output_cotangent: bfloat16 [8192, 2048], P('fs', 'tp'), may hold values from -50 to 50
- output_factor: bfloat16 [1024, 128], replicated, may hold values from -10 to 10
- output_master: float32 [1024, 2048], P('fs', 'tp'), may hold values from -0.1875 to 0.1875
- output_first: float32 [128, 2048], P('fs', 'tp'), may hold values from -4 to 4
- output_second: float32 [128, 2048], P('fs', 'tp'), may hold values from 0.01 to 0.2
Outputs:
- value_step: float32 [512, 2048], P('fs', 'tp')
- value_new_master: float32 [512, 2048], P('fs', 'tp')
- value_copy: bfloat16 [512, 2048], P(None, 'tp')
- value_first_new: float32 [128, 2048], P('fs', 'tp')
- value_second_new: float32 [128, 2048], P('fs', 'tp')
- output_step: float32 [1024, 2048], P('fs', 'tp')
- output_new_master: float32 [1024, 2048], P('fs', 'tp')
- output_copy: bfloat16 [1024, 2048], P(None, 'tp')
- output_first_new: float32 [128, 2048], P('fs', 'tp')
- output_second_new: float32 [128, 2048], P('fs', 'tp')
All inputs are finite; a program needn't handle non-finite values.
Results may differ from a plain program's by a relative error of at most 0.001.
Values may be sent and summed in bfloat16 or wider, within the bound.
A program may use at most 64 MiB of HBM per device.

v0:
```python
import jax
import jax.numpy as jnp
from jax import lax
from jax.sharding import PartitionSpec as P

highest = lax.Precision.HIGHEST


def tokens_exact(left, right):
    return lax.dot_general(
        left, right, (((0,), (0,)), ((), ())), precision=highest, preferred_element_type=jnp.float32
    )


def moment_update(projected, scale, first, second):
    scaled = scale * projected
    first_new = 0.9 * first + 0.1 * scaled
    second_new = 0.95 * second + 0.05 * scaled * scaled
    direction = first_new / (jnp.sqrt(second_new) + 1e-08)
    return (first_new, second_new, direction)


def project_both(value_image, output_image, value_input, output_cotangent, band):
    value_wide = value_input.astype(jnp.float32)
    output_wide = output_cotangent.astype(jnp.float32)
    columns = value_input.shape[1]
    blocks = lax.axis_size("fs") * (2 * band) // (2 * band)
    value_term = tokens_exact(value_image, value_wide).reshape(blocks, band, columns)
    output_term = tokens_exact(output_image, output_wide).reshape(blocks, band, columns)
    paired = lax.psum_scatter(
        jnp.stack([value_term, output_term], axis=1).reshape(
            lax.axis_size("fs") * (2 * band), columns
        ),
        "fs",
        scatter_dimension=0,
        tiled=True,
    )
    return (paired[:band], paired[band:])


def on_device(
    value_input,
    value_cotangent,
    value_factor,
    value_master,
    value_first,
    value_second,
    mixed_heads,
    output_cotangent,
    output_factor,
    output_master,
    output_first,
    output_second,
):
    fs_count = lax.axis_size("fs")
    fs_place = lax.axis_index("fs")
    rank = value_factor.shape[1]
    band = rank // fs_count
    columns = value_input.shape[1]
    value_rows = value_master.shape[0]
    output_rows = output_master.shape[0]
    value_block = lax.dynamic_slice_in_dim(
        value_factor, fs_place * value_rows, value_rows, 0
    ).astype(jnp.float32)
    output_block = lax.dynamic_slice_in_dim(
        output_factor, fs_place * output_rows, output_rows, 0
    ).astype(jnp.float32)
    value_image = jnp.dot(value_cotangent, value_factor, preferred_element_type=jnp.float32)
    heads_whole = lax.all_gather(mixed_heads, "tp", axis=1, tiled=True)
    output_image = jnp.dot(heads_whole, output_factor, preferred_element_type=jnp.float32)
    value_proj, output_proj = project_both(
        value_image, output_image, value_input, output_cotangent, band
    )
    total_count = rank * columns * lax.axis_size("tp")
    value_square, output_square = lax.psum(
        (jnp.sum(value_proj * value_proj), jnp.sum(output_proj * output_proj)), ("fs", "tp")
    )
    value_scale = lax.rsqrt(value_square / total_count + 1e-06)
    output_scale = lax.rsqrt(output_square / total_count + 1e-06)
    value_first_new, value_second_new, value_dir = moment_update(
        value_proj, value_scale, value_first, value_second
    )
    output_first_new, output_second_new, output_dir = moment_update(
        output_proj, output_scale, output_first, output_second
    )
    value_dir_all, output_dir_all = (
        lax.all_gather(value_dir, "fs", axis=0, tiled=True),
        lax.all_gather(output_dir, "fs", axis=0, tiled=True),
    )
    value_step = jnp.dot(
        value_block, value_dir_all, precision=highest, preferred_element_type=jnp.float32
    )
    output_step = jnp.dot(
        output_block, output_dir_all, precision=highest, preferred_element_type=jnp.float32
    )
    value_new = value_master - 0.002 * value_step
    output_new = output_master - 0.002 * output_step
    value_copy, output_copy = (
        lax.all_gather(value_new.astype(jnp.bfloat16), "fs", axis=0, tiled=True),
        lax.all_gather(output_new.astype(jnp.bfloat16), "fs", axis=0, tiled=True),
    )
    return (
        value_step,
        value_new,
        value_copy,
        value_first_new,
        value_second_new,
        output_step,
        output_new,
        output_copy,
        output_first_new,
        output_second_new,
    )


def solution(mesh):
    in_specs = (
        P("fs", "tp"),
        P("fs", None),
        P(),
        P("fs", "tp"),
        P("fs", "tp"),
        P("fs", "tp"),
        P("fs", "tp"),
        P("fs", "tp"),
        P(),
        P("fs", "tp"),
        P("fs", "tp"),
        P("fs", "tp"),
    )
    out_specs = (
        P("fs", "tp"),
        P("fs", "tp"),
        P(None, "tp"),
        P("fs", "tp"),
        P("fs", "tp"),
        P("fs", "tp"),
        P("fs", "tp"),
        P(None, "tp"),
        P("fs", "tp"),
        P("fs", "tp"),
    )
    return jax.shard_map(
        on_device, mesh=mesh, in_specs=in_specs, out_specs=out_specs, check_vma=False
    )
```

profile of v0, /device:TPU:0, one launch (start us, length us, event | category | flops | bytes accessed | tf_op | source)
XLA Modules:
  0.0 180.0 jit_solution(13130348635020009282)
XLA Ops:
  7.2 0.0 copy-start
  7.2 0.0 copy-start.1
  7.2 0.0 copy-start.3
  7.2 0.0 all-gather.2.cloned.1.call-start
  7.3 0.7 all-gather.2.cloned.1.call-update
  7.9 0.0 reduce-scatter.2.cloned.1.call-start
  8.0 0.8 copy-done
  8.8 1.6 fusion.12
  10.4 0.0 copy-done.1
  10.4 1.0 fusion.13
  11.4 0.0 copy-start.2
  11.4 48.8 %all-gather.2.cloned.1.call-done = bf16[2048,1024]{1,0:T(8,128)(2,1)} async-done(((bf16[2048,128]{1,0:T(8,128)(2,1)}), bf16[2048,1024]{1,0:T(8,128)(2,1)}) %all-gather.2.cloned.1.call-update) | async-done | bytes 4194320 | tf_op jit(solution)/shard_map/all_gather | solution.py:69
  60.2 0.0 copy-done.3
  60.2 3.5 %fusion.14 = f32[2048,128]{1,0:T(8,128)S(1)} fusion(bf16[2048,1024]{1,0:T(8,128)(2,1)} %all-gather.2.cloned.1.call-done, bf16[1024,128]{1,0:T(8,128)(2,1)S(1)} %copy-done.3), kind=kOutput, calls=%fused_computation.25 | convolution fusion | flops 536870912 | bytes 5505024 | tf_op jit(solution)/shard_map/dot_general | solution.py:70
  63.7 0.0 copy-done.2
  63.7 1.0 fusion.15
  64.7 0.7 copy.22
  65.5 0.0 reduce-scatter.2.cloned.1.call-update
  65.5 22.7 %reduce-scatter.2.cloned.1.call-done = f32[64,256]{1,0:T(8,128)} async-done(((f32[256,256]{1,0:T(8,128)}), f32[64,256]{1,0:T(8,128)}) %reduce-scatter.2.cloned.1.call-update) | async-done | bytes 65552 | tf_op jit(solution)/shard_map/reduce_scatter | solution.py:30
  88.2 1.4 multiply_reduce_fusion
  89.6 39.5 %all-reduce = (f32[]{:T(128)}, f32[]{:T(128)}) all-reduce(f32[]{:T(128)} %get-tuple-element.11, f32[]{:T(128)} %get-tuple-element.10), channel_id=1, replica_groups=mesh['fs'=4,'tp'=8] {'fs','tp'}, use_global_device_ids=true, to_apply=%region_2.0 | all-reduce | flops 2 | bytes 16 | tf_op jit(solution)/shard_map/psum | solution.py:75
  130.5 1.5 add_divide_fusion
  132.0 9.4 %all_gather.18 = f32[128,256]{1,0:T(8,128)S(1)} all-gather(f32[32,256]{1,0:T(8,128)S(1)} %get-tuple-element.16), channel_id=1, replica_groups=mesh['fs'=4,'tp'=8] {'fs'}, dimensions={0}, use_global_device_ids=true | all-gather | bytes 163840 | tf_op jit(solution)/shard_map/all_gather | solution.py:88
  141.4 2.0 %fusion.8 = (bf16[256,256]{1,0:T(8,128)(2,1)S(1)}, f32[256,256]{1,0:T(8,128)}, f32[256,256]{1,0:T(8,128)}) fusion(f32[256,256]{1,0:T(8,128)} %param.21, f32[128,256]{1,0:T(8,128)S(1)} %all_gather.18, bf16[1024,128]{1,0:T(8,128)(2,1)S(1)} %copy-done.3, s32[]{:T(128)S(6)} %select_n.7), kind=kOutput, calls=%fused_computation.21 | convolution fusion | flops 100859904 | bytes 1114116 | tf_op jit(solution)/shard_map/dot_general | solution.py:93
  143.4 10.0 %all_gather.19 = bf16[1024,256]{1,0:T(8,128)(2,1)S(1)} all-gather(bf16[256,256]{1,0:T(8,128)(2,1)S(1)} %get-tuple-element.14), channel_id=1, replica_groups=mesh['fs'=4,'tp'=8] {'fs'}, dimensions={0}, use_global_device_ids=true | all-gather | bytes 655360 | tf_op jit(solution)/shard_map/all_gather | solution.py:100
  153.4 7.7 %all_gather.16 = f32[128,256]{1,0:T(8,128)S(1)} all-gather(f32[32,256]{1,0:T(8,128)S(1)} %get-tuple-element.24), channel_id=1, replica_groups=mesh['fs'=4,'tp'=8] {'fs'}, dimensions={0}, use_global_device_ids=true | all-gather | bytes 163840 | tf_op jit(solution)/shard_map/all_gather | solution.py:87
  161.0 1.8 %fusion.10 = (bf16[128,256]{1,0:T(8,128)(2,1)S(1)}, f32[128,256]{1,0:T(8,128)}, f32[128,256]{1,0:T(8,128)}) fusion(f32[128,256]{1,0:T(8,128)} %param.15, f32[128,256]{1,0:T(8,128)S(1)} %all_gather.16, bf16[512,128]{1,0:T(8,128)(2,1)} %param.14, s32[]{:T(128)S(6)} %select_n.6), kind=kOutput, calls=%fused_computation.22 | convolution fusion | flops 50429952 | bytes 622596 | tf_op jit(solution)/shard_map/dot_general | solution.py:90
  162.9 8.8 %all_gather.17 = bf16[512,256]{1,0:T(8,128)(2,1)S(1)} all-gather(bf16[128,256]{1,0:T(8,128)(2,1)S(1)} %get-tuple-element.19), channel_id=1, replica_groups=mesh['fs'=4,'tp'=8] {'fs'}, dimensions={0}, use_global_device_ids=true | all-gather | bytes 327680 | tf_op jit(solution)/shard_map/all_gather | solution.py:99
  171.6 0.7 copy.25
  172.3 0.8 copy.26
  (1 shorter events, 0.0 us)
Async XLA Ops:
  7.2 1.6 copy-start
  7.2 3.2 %copy-start.1 = (bf16[2048,256]{1,0:T(8,128)(2,1)S(1)}, bf16[2048,256]{1,0:T(8,128)(2,1)}, u32[]{:S(2)}) copy-start(bf16[2048,256]{1,0:T(8,128)(2,1)} %param.12) | copy-start | bytes 3145732
  7.2 53.0 %copy-start.3 = (bf16[1024,128]{1,0:T(8,128)(2,1)S(1)}, bf16[1024,128]{1,0:T(8,128)(2,1)}, u32[]{:S(2)}) copy-start(bf16[1024,128]{1,0:T(8,128)(2,1)} %param.20) | copy-start | bytes 786436
  7.2 53.0 %all-gather.2.cloned.1.call-start = ((), (), s32[]{:S(2)}) async-start(), calls=%async_computation.1 | async-start | bytes 4718592 | tf_op jit(solution)/shard_map/all_gather | solution.py:69
  7.9 80.2 %reduce-scatter.2.cloned.1.call-start = ((), (), s32[]{:S(2)}) async-start(), calls=%async_computation.2 | async-start | bytes 327680 | tf_op jit(solution)/shard_map/reduce_scatter | solution.py:30
  11.4 52.3 %copy-start.2 = (bf16[2048,256]{1,0:T(8,128)(2,1)S(1)}, bf16[2048,256]{1,0:T(8,128)(2,1)}, u32[]{:S(2)}) copy-start(bf16[2048,256]{1,0:T(8,128)(2,1)} %param.19) | copy-start | bytes 3145732
Sparse Core Ops, SparseCore 0:
  9.6 50.5 all-gather.1
  65.6 22.5 reduce-scatter.1
where the time goes:
time: 180 us
  blocking collectives  75.3 us (42%)
  waiting for transfers between devices  72.2 us (40%)
  between operations  15.5 us (9%)
  matrix products  10.9 us (6%)
  local copies, waits for them, and re-layouts  3.02 us (2%)
  other arithmetic  2.93 us (2%)
    all_gather x1, waiting for transfers between devices, on_device(): heads_whole = lax.all_gather(mixed_heads, 'tp', axis=1, tiled=True)  48.8 us
    psum x1, blocking collectives, on_device(): lax.psum((jnp.sum(value_proj * value_proj), jnp.sum(output_proj * output_...  39.5 us
    reduce_scatter x1, waiting for transfers between devices, project_both(): lax.psum_scatter(jnp.stack([value_term, output_term], axis=1).reshape(lax...  22.7 us
    all_gather x1, blocking collectives, on_device(): lax.all_gather(output_new.astype(jnp.bfloat16), 'fs', axis=0, tiled=True)  9.99 us
    all_gather x1, blocking collectives, on_device(): lax.all_gather(output_dir, 'fs', axis=0, tiled=True)  9.39 us
    all_gather x1, blocking collectives, on_device(): lax.all_gather(value_new.astype(jnp.bfloat16), 'fs', axis=0, tiled=True)  8.76 us
    all_gather x1, blocking collectives, on_device(): lax.all_gather(value_dir, 'fs', axis=0, tiled=True)  7.66 us
  transfers between devices with their start and end apart: 2, of which 2 were waited for; matrix products, arithmetic and copies ran while one was open for 1% of the time, Pallas kernels for 0%

commit v1 on v0

--- a/solution.py
+++ b/solution.py
@@ -73,7 +73,7 @@
     )
     total_count = rank * columns * lax.axis_size("tp")
     value_square, output_square = lax.psum(
-        (jnp.sum(value_proj * value_proj), jnp.sum(output_proj * output_proj)), ("fs", "tp")
+        lax.psum((jnp.sum(value_proj * value_proj), jnp.sum(output_proj * output_proj)), "tp"), "fs"
     )
     value_scale = lax.rsqrt(value_square / total_count + 1e-06)
     output_scale = lax.rsqrt(output_square / total_count + 1e-06)

time: 180 us -> 166 us (0.922)
  blocking collectives: 75.3 us -> 60.4 us
    psum x1, blocking collectives: 39.5 us -> 16.4 us  [on_device(): lax.psum((jnp.sum(value_proj * value_proj), jnp.sum(output_proj * output_...]
    psum x0 -> x1, blocking collectives: none -> 9.74 us  [on_device(): lax.psum(lax.psum((jnp.sum(value_proj * value_proj), jnp.sum(output_proj...]
  transfers between devices with their start and end apart: 2 -> 2, of which waited for: 2 -> 2; matrix products, arithmetic and copies ran while one was open for 1% -> 2% of each run, Pallas kernels for 0% -> 0%
where the time goes in v1:
time: 166 us; the launch traced here: 165 us
  waiting for transfers between devices  72.2 us (43%)
  blocking collectives  60.4 us (36%)
  between operations  15.5 us (9%)
  matrix products  10.9 us (7%)
  local copies, waits for them, and re-layouts  3.02 us (2%)
  other arithmetic  2.93 us (2%)
    all_gather x1, waiting for transfers between devices, on_device(): heads_whole = lax.all_gather(mixed_heads, 'tp', axis=1, tiled=True)  48.8 us
    reduce_scatter x1, waiting for transfers between devices, project_both(): lax.psum_scatter(jnp.stack([value_term, output_term], axis=1).reshape(lax...  22.7 us
    psum x1, blocking collectives, on_device(): lax.psum((jnp.sum(value_proj * value_proj), jnp.sum(output_proj * output_...  16.4 us
    psum x1, blocking collectives, on_device(): lax.psum(lax.psum((jnp.sum(value_proj * value_proj), jnp.sum(output_proj...  9.74 us
    all_gather x1, blocking collectives, on_device(): lax.all_gather(output_new.astype(jnp.bfloat16), 'fs', axis=0, tiled=True)  9.11 us
    all_gather x1, blocking collectives, on_device(): lax.all_gather(output_dir, 'fs', axis=0, tiled=True)  8.74 us
    all_gather x1, blocking collectives, on_device(): lax.all_gather(value_dir, 'fs', axis=0, tiled=True)  8.37 us
    all_gather x1, blocking collectives, on_device(): lax.all_gather(value_new.astype(jnp.bfloat16), 'fs', axis=0, tiled=True)  8.05 us
  transfers between devices with their start and end apart: 2, of which 2 were waited for; matrix products, arithmetic and copies ran while one was open for 2% of the time, Pallas kernels for 0%

profile of v1, /device:TPU:0, one launch (start us, length us, event | category | flops | bytes accessed | tf_op | source)
XLA Modules:
  0.0 165.1 jit_solution(15707612821833642794)
XLA Ops:
  7.2 0.0 copy-start
  7.2 0.0 copy-start.1
  7.2 0.0 copy-start.3
  7.2 0.0 all-gather.2.cloned.1.call-start
  7.3 0.7 all-gather.2.cloned.1.call-update
  7.9 0.0 reduce-scatter.2.cloned.1.call-start
  8.0 0.8 copy-done
  8.8 1.6 fusion.12
  10.4 0.0 copy-done.1
  10.4 1.0 fusion.13
  11.4 0.0 copy-start.2
  11.4 48.8 %all-gather.2.cloned.1.call-done = bf16[2048,1024]{1,0:T(8,128)(2,1)} async-done(((bf16[2048,128]{1,0:T(8,128)(2,1)}), bf16[2048,1024]{1,0:T(8,128)(2,1)}) %all-gather.2.cloned.1.call-update) | async-done | bytes 4194320 | tf_op jit(solution)/shard_map/all_gather | solution.py:69
  60.2 0.0 copy-done.3
  60.2 3.5 %fusion.14 = f32[2048,128]{1,0:T(8,128)S(1)} fusion(bf16[2048,1024]{1,0:T(8,128)(2,1)} %all-gather.2.cloned.1.call-done, bf16[1024,128]{1,0:T(8,128)(2,1)S(1)} %copy-done.3), kind=kOutput, calls=%fused_computation.25 | convolution fusion | flops 536870912 | bytes 5505024 | tf_op jit(solution)/shard_map/dot_general | solution.py:70
  63.7 0.0 copy-done.2
  63.7 1.0 fusion.15
  64.7 0.7 copy.22
  65.5 0.0 reduce-scatter.2.cloned.1.call-update
  65.5 22.7 %reduce-scatter.2.cloned.1.call-done = f32[64,256]{1,0:T(8,128)} async-done(((f32[256,256]{1,0:T(8,128)}), f32[64,256]{1,0:T(8,128)}) %reduce-scatter.2.cloned.1.call-update) | async-done | bytes 65552 | tf_op jit(solution)/shard_map/reduce_scatter | solution.py:30
  88.2 1.4 multiply_reduce_fusion
  89.6 16.4 %all-reduce = (f32[]{:T(128)}, f32[]{:T(128)}) all-reduce(f32[]{:T(128)} %get-tuple-element.11, f32[]{:T(128)} %get-tuple-element.10), channel_id=1, replica_groups=mesh['fs'=4,'tp'=8] {'tp'}, use_global_device_ids=true, to_apply=%region_2.0 | all-reduce | flops 2 | bytes 16 | tf_op jit(solution)/shard_map/psum | solution.py:76
  106.0 9.7 %all-reduce.1 = (f32[]{:T(128)}, f32[]{:T(128)}) all-reduce(f32[]{:T(128)} %get-tuple-element.12, f32[]{:T(128)} %get-tuple-element.13), channel_id=1, replica_groups=mesh['fs'=4,'tp'=8] {'fs'}, use_global_device_ids=true, to_apply=%region_3.0 | all-reduce | flops 2 | bytes 16 | tf_op jit(solution)/shard_map/psum | solution.py:75
  117.1 1.5 add_divide_fusion
  118.6 8.7 %all_gather.18 = f32[128,256]{1,0:T(8,128)S(1)} all-gather(f32[32,256]{1,0:T(8,128)S(1)} %get-tuple-element.18), channel_id=1, replica_groups=mesh['fs'=4,'tp'=8] {'fs'}, dimensions={0}, use_global_device_ids=true | all-gather | bytes 163840 | tf_op jit(solution)/shard_map/all_gather | solution.py:88
  127.4 2.0 %fusion.8 = (bf16[256,256]{1,0:T(8,128)(2,1)S(1)}, f32[256,256]{1,0:T(8,128)}, f32[256,256]{1,0:T(8,128)}) fusion(f32[256,256]{1,0:T(8,128)} %param.21, f32[128,256]{1,0:T(8,128)S(1)} %all_gather.18, bf16[1024,128]{1,0:T(8,128)(2,1)S(1)} %copy-done.3, s32[]{:T(128)S(6)} %select_n.7), kind=kOutput, calls=%fused_computation.21 | convolution fusion | flops 100859904 | bytes 1114116 | tf_op jit(solution)/shard_map/dot_general | solution.py:93
  129.4 9.1 %all_gather.19 = bf16[1024,256]{1,0:T(8,128)(2,1)S(1)} all-gather(bf16[256,256]{1,0:T(8,128)(2,1)S(1)} %get-tuple-element.16), channel_id=1, replica_groups=mesh['fs'=4,'tp'=8] {'fs'}, dimensions={0}, use_global_device_ids=true | all-gather | bytes 655360 | tf_op jit(solution)/shard_map/all_gather | solution.py:100
  138.5 8.4 %all_gather.16 = f32[128,256]{1,0:T(8,128)S(1)} all-gather(f32[32,256]{1,0:T(8,128)S(1)} %get-tuple-element.26), channel_id=1, replica_groups=mesh['fs'=4,'tp'=8] {'fs'}, dimensions={0}, use_global_device_ids=true | all-gather | bytes 163840 | tf_op jit(solution)/shard_map/all_gather | solution.py:87
  146.8 1.8 %fusion.10 = (bf16[128,256]{1,0:T(8,128)(2,1)S(1)}, f32[128,256]{1,0:T(8,128)}, f32[128,256]{1,0:T(8,128)}) fusion(f32[128,256]{1,0:T(8,128)} %param.15, f32[128,256]{1,0:T(8,128)S(1)} %all_gather.16, bf16[512,128]{1,0:T(8,128)(2,1)} %param.14, s32[]{:T(128)S(6)} %select_n.6), kind=kOutput, calls=%fused_computation.22 | convolution fusion | flops 50429952 | bytes 622596 | tf_op jit(solution)/shard_map/dot_general | solution.py:90
  148.7 8.1 %all_gather.17 = bf16[512,256]{1,0:T(8,128)(2,1)S(1)} all-gather(bf16[128,256]{1,0:T(8,128)(2,1)S(1)} %get-tuple-element.21), channel_id=1, replica_groups=mesh['fs'=4,'tp'=8] {'fs'}, dimensions={0}, use_global_device_ids=true | all-gather | bytes 327680 | tf_op jit(solution)/shard_map/all_gather | solution.py:99
  156.7 0.7 copy.25
  157.4 0.8 copy.26
  (1 shorter events, 0.0 us)
Async XLA Ops:
  7.2 1.6 copy-start
  7.2 3.2 %copy-start.1 = (bf16[2048,256]{1,0:T(8,128)(2,1)S(1)}, bf16[2048,256]{1,0:T(8,128)(2,1)}, u32[]{:S(2)}) copy-start(bf16[2048,256]{1,0:T(8,128)(2,1)} %param.12) | copy-start | bytes 3145732
  7.2 53.0 %copy-start.3 = (bf16[1024,128]{1,0:T(8,128)(2,1)S(1)}, bf16[1024,128]{1,0:T(8,128)(2,1)}, u32[]{:S(2)}) copy-start(bf16[1024,128]{1,0:T(8,128)(2,1)} %param.20) | copy-start | bytes 786436
  7.2 53.0 %all-gather.2.cloned.1.call-start = ((), (), s32[]{:S(2)}) async-start(), calls=%async_computation.1 | async-start | bytes 4718592 | tf_op jit(solution)/shard_map/all_gather | solution.py:69
  7.9 80.2 %reduce-scatter.2.cloned.1.call-start = ((), (), s32[]{:S(2)}) async-start(), calls=%async_computation.2 | async-start | bytes 327680 | tf_op jit(solution)/shard_map/reduce_scatter | solution.py:30
  11.4 52.3 %copy-start.2 = (bf16[2048,256]{1,0:T(8,128)(2,1)S(1)}, bf16[2048,256]{1,0:T(8,128)(2,1)}, u32[]{:S(2)}) copy-start(bf16[2048,256]{1,0:T(8,128)(2,1)} %param.19) | copy-start | bytes 3145732
Sparse Core Ops, SparseCore 0:
  9.6 50.5 all-gather.1
  65.6 22.5 reduce-scatter.1
